TPU v7x, 256 devices: a whole 4x4x8 slice. The times are simulated.
256 devices in a mesh: ep: 128 (over z, y, x), tp: 2 (over core).
Axes of the slice: x: 4, y: 4, z: 8, core: 2. Of those that a mesh axis runs over, the one named last changes fastest.
Arguments:
- resid: bfloat16 [2048, 2048], P('ep'), may hold values from -6 to 6
- proj_x: bfloat16 [2048, 2048], P('ep', 'tp'), may hold values from -6 to 6
- proj_z: bfloat16 [2048, 2048], P('ep', 'tp'), may hold values from -6 to 6
- proj_bc: bfloat16 [2048, 2, 512], P('ep', None, 'tp'), may hold values from -6 to 6
- proj_dt: bfloat16 [2048, 32], P('ep', 'tp'), may hold values from -6 to 6
- tail_x: bfloat16 [2048, 3, 2048], P('ep', None, 'tp'), may hold values from -6 to 6
- tail_bc: bfloat16 [2048, 3, 2, 512], P('ep', None, None, 'tp'), may hold values from -6 to 6
- taps_x: bfloat16 [4, 2048], P(None, 'tp'), may hold values from -3 to 3
- taps_bc: bfloat16 [4, 2, 512], P(None, None, 'tp'), may hold values from -3 to 3
- ssm_state: float32 [2048, 32, 4096], P('ep', 'tp'), may hold values from -1.5 to 1.5
- dt_bias: float32 [32], P('tp'), may hold values from -4 to 0
- decay_log: float32 [32], P('tp'), may hold values from -1 to 2.5
- group_gain: float32 [2048], P('tp'), may hold values from 0.1 to 1.9
- out_proj: bfloat16 [2048, 2048], P('tp', 'ep'), may hold values from -0.125 to 0.125
- ffn_gain: float32 [2048], replicated, may hold values from 0.1 to 1.9
- dense_gate: bfloat16 [2048, 4096], P(None, ('ep', 'tp')), may hold values from -0.125 to 0.125
- dense_up: bfloat16 [2048, 4096], P(None, ('ep', 'tp')), may hold values from -0.125 to 0.125
- dense_down: bfloat16 [4096, 2048], P(('ep', 'tp')), may hold values from -0.09375 to 0.09375
- branch_gate: bfloat16 [2048], replicated, may hold values from -0.125 to 0.125
- group_weights: float32 [2048, 4], replicated, may hold values from 0.2 to 1
- expert_ids: int32 [2048, 6], replicated, may hold values from 0 to 127, all different within a row; in each aligned block of 16 rows (0 to 15, 16 to 31, ...) at most 2 rows name the same one
- expert_weights: float32 [2048, 6], replicated, may hold values from 0.1 to 1
- exp_gate: bfloat16 [128, 2048, 512], P('ep', None, 'tp'), may hold values from -0.125 to 0.125
- exp_up: bfloat16 [128, 2048, 512], P('ep', None, 'tp'), may hold values from -0.125 to 0.125
- exp_down: bfloat16 [128, 512, 2048], P('ep', 'tp'), may hold values from -0.25 to 0.25
Outputs:
- out: bfloat16 [2048, 2048], P(('ep', 'tp'))
- new_state: float32 [2048, 32, 4096], P('ep', 'tp')
Inputs may be any that keep to these rules, and one draw needn't show every extreme that they name: `expert_ids`: each row names 6 different experts. In the rows of one index of ep (aligned blocks of 16 rows) no expert is named more than 2 times, a bound that some block reaches.
All inputs are finite; a program needn't handle non-finite values.
Results may differ from a plain program's by a relative error of at most 0.013.
Values may be sent and summed in bfloat16 or wider, within the bound.
A program may use at most 128 MiB of HBM per device.

v0:
```python
import jax
import jax.numpy as jnp
from jax import lax
from jax.sharding import Mesh
from jax.sharding import PartitionSpec as P

HEAD_P = 64
NSTATE = 64
GROUPS = 4
TOPK = 6
HPG = 4
EP = ("ep_0", "ep_1", "ep_2")
EP_TP = ("ep_0", "ep_1", "ep_2", "tp")
EPSILON = 1e-06


def gathered_by_axis(shard, axes, dim):
    if not axes:
        return shard
    nearer = lax.all_gather(shard, axes[-1], axis=dim, tiled=True)
    return gathered_by_axis(nearer, axes[:-1], dim)


def sent_to_all(shard, axis):
    copies = jnp.broadcast_to(shard, (lax.axis_size(axis), *shard.shape))
    return lax.all_to_all(copies, axis, split_axis=0, concat_axis=0, tiled=True)


def of_everyone(shard, axis):
    everything = sent_to_all(shard, axis)
    return jnp.sum(everything.astype(jnp.float32), axis=0)


def split_up(shard, dim, devices):
    before, after = (shard.shape[:dim], shard.shape[dim + 1 :])
    return jnp.moveaxis(shard.reshape(*before, devices, -1, *after), dim, 0)


def sum_at_owner(shard, axis, dim):
    devices = lax.axis_size(axis)
    pieces = lax.all_to_all(split_up(shard, dim, devices), axis, 0, 0, tiled=True)
    return jnp.sum(pieces.astype(jnp.float32), axis=0)


def summed_rows(shard, axes, dim):
    far, near = axes
    pieces = split_up(shard, dim, lax.axis_size(far))
    nearer = sum_at_owner(pieces, near, dim + 1)
    arrived = lax.all_to_all(
        nearer.astype(jnp.bfloat16), far, split_axis=0, concat_axis=0, tiled=True
    )
    return arrived.astype(jnp.float32).sum(axis=0)


def state_update(
    proj_x,
    proj_z,
    proj_bc,
    proj_dt,
    tail_x,
    tail_bc,
    taps_x,
    taps_bc,
    ssm_state,
    dt_bias,
    decay_log,
    group_gain,
):
    window_x = jnp.concatenate([tail_x, proj_x[:, None]], axis=1).astype(jnp.float32)
    conv_x = jax.nn.silu(jnp.sum(window_x * taps_x.astype(jnp.float32)[None], axis=1))
    window_bc = jnp.concatenate([tail_bc, proj_bc[:, None]], axis=1).astype(jnp.float32)
    conv_bc = jax.nn.silu(jnp.sum(window_bc * taps_bc.astype(jnp.float32)[None], axis=1))
    count = proj_x.shape[0]
    heads = proj_dt.shape[1]
    x_heads = conv_x.reshape(count, heads, HEAD_P)
    grouped_bc = conv_bc.reshape(count, 2, heads // HPG, NSTATE)
    input_heads = jnp.repeat(grouped_bc[:, 0], HPG, axis=1)
    read_heads = jnp.repeat(grouped_bc[:, 1], HPG, axis=1)
    step_size = jax.nn.softplus(proj_dt.astype(jnp.float32) + dt_bias)
    decay = jnp.exp(-step_size * jnp.exp(decay_log))
    state = ssm_state.reshape(count, heads, HEAD_P, NSTATE)
    fresh = (step_size[:, :, None] * x_heads)[:, :, :, None] * input_heads[:, :, None, :]
    new_state = decay[:, :, None, None] * state + fresh
    readout = jnp.sum(new_state * read_heads[:, :, None, :], axis=-1)
    gated = readout.reshape(count, heads * HEAD_P) * jax.nn.silu(proj_z.astype(jnp.float32))
    grouped = gated.reshape(count, heads // HPG, HPG * HEAD_P)
    grouped = grouped * lax.rsqrt(jnp.mean(grouped * grouped, axis=-1, keepdims=True) + EPSILON)
    y_out = (grouped.reshape(count, heads * HEAD_P) * group_gain).astype(jnp.bfloat16)
    return (y_out, new_state.reshape(count, heads, HEAD_P * NSTATE))


def shards(
    resid,
    proj_x,
    proj_z,
    proj_bc,
    proj_dt,
    tail_x,
    tail_bc,
    taps_x,
    taps_bc,
    ssm_state,
    dt_bias,
    decay_log,
    group_gain,
    out_proj,
    ffn_gain,
    dense_gate,
    dense_up,
    dense_down,
    branch_gate,
    group_weights,
    expert_ids,
    expert_weights,
    exp_gate,
    exp_up,
    exp_down,
):
    y_out, new_state = state_update(
        proj_x,
        proj_z,
        proj_bc,
        proj_dt,
        tail_x,
        tail_bc,
        taps_x,
        taps_bc,
        ssm_state,
        dt_bias,
        decay_log,
        group_gain,
    )
    partial_value = jnp.dot(
        y_out, gathered_by_axis(out_proj, EP, 1), preferred_element_type=jnp.float32
    )
    mixed = of_everyone(partial_value.astype(jnp.bfloat16), "tp").astype(jnp.float32)
    resid_new = (resid.astype(jnp.float32) + mixed).astype(jnp.bfloat16)
    widened = resid_new.astype(jnp.float32)
    normed = (
        widened
        * lax.rsqrt(jnp.mean(widened * widened, axis=-1, keepdims=True) + EPSILON)
        * ffn_gain
    ).astype(jnp.bfloat16)
    gathered = lax.all_gather(normed, EP, axis=0, tiled=True)
    score = jnp.dot(gathered, branch_gate, preferred_element_type=jnp.float32)
    dense_pre = jnp.dot(gathered, dense_gate, preferred_element_type=jnp.float32)
    dense_lin = jnp.dot(gathered, dense_up, preferred_element_type=jnp.float32)
    dense_hidden = (jax.nn.sigmoid(score)[:, None] * jax.nn.silu(dense_pre) * dense_lin).astype(
        jnp.bfloat16
    )
    experts = lax.axis_size(EP)
    expert_own = lax.axis_index(EP)
    cores = lax.axis_size("tp")
    core_index = lax.axis_index("tp")
    batch = gathered.shape[0]
    rows_each = batch // experts
    half_rows = rows_each // cores
    pairs = rows_each * TOPK
    capacity = (pairs + experts - 1) // experts + 1
    group_size = experts // GROUPS
    levels = jnp.arange(1, capacity + 1, dtype=jnp.int32)
    pair_row = jnp.arange(pairs, dtype=jnp.int32) // TOPK
    pick = (jnp.arange(GROUPS, dtype=jnp.int32) == expert_own // group_size).astype(jnp.float32)
    coarse = jnp.sum(group_weights * pick[None], axis=1)
    pair_weight = (expert_weights * coarse[:, None]).reshape(experts, pairs)
    hits = (expert_ids.reshape(experts, pairs) == expert_own).astype(jnp.int32)
    ranks = jnp.cumsum(hits, axis=1, dtype=jnp.int32)
    select = hits[:, None, :] * (ranks[:, None, :] == levels[None, :, None]).astype(jnp.int32)
    local_row = jnp.sum(select * pair_row[None, None, :], axis=-1, dtype=jnp.int32)
    filled = jnp.sum(select, axis=-1, dtype=jnp.int32).reshape(-1)
    slot_weight = jnp.sum(select.astype(jnp.float32) * pair_weight[:, None, :], axis=-1).reshape(-1)
    row_index = (local_row + jnp.arange(experts, dtype=jnp.int32)[:, None] * rows_each).reshape(-1)
    slot_rows = jnp.take(gathered, row_index, axis=0)
    slot_pre = jnp.dot(slot_rows, exp_gate[0], preferred_element_type=jnp.float32)
    slot_lin = jnp.dot(slot_rows, exp_up[0], preferred_element_type=jnp.float32)
    slot_hidden = (slot_weight[:, None] * jax.nn.silu(slot_pre) * slot_lin).astype(jnp.bfloat16)
    placing = (jnp.arange(batch, dtype=jnp.int32)[:, None] == row_index[None, :]) & (
        filled[None, :] > 0
    )
    row_hidden = jnp.dot(
        placing.astype(jnp.bfloat16), slot_hidden, preferred_element_type=jnp.float32
    ).astype(jnp.bfloat16)
    joined = jnp.concatenate([dense_hidden, row_hidden], axis=1)
    down_all = jnp.concatenate([dense_down, exp_down[0]], axis=0)
    inner_width = joined.shape[1]
    ordered = (
        joined.reshape(experts, cores, half_rows, inner_width)
        .transpose(1, 0, 2, 3)
        .reshape(batch, inner_width)
    )
    halved = sum_at_owner(
        jnp.dot(ordered, down_all, preferred_element_type=jnp.float32).astype(jnp.bfloat16), "tp", 0
    )
    branch = summed_rows(halved.astype(jnp.bfloat16), ("ep_0", ("ep_1", "ep_2")), 0)
    own_rows = lax.dynamic_slice_in_dim(widened, core_index * half_rows, half_rows, 0)
    out = (own_rows + branch).astype(jnp.bfloat16)
    return (out, new_state)


def solution(mesh):
    finer = Mesh(mesh.devices.reshape(8, 4, 4, mesh.shape["tp"]), ("ep_0", "ep_1", "ep_2", "tp"))
    in_specs = (
        P(EP, None),
        P(EP, "tp"),
        P(EP, "tp"),
        P(EP, None, "tp"),
        P(EP, "tp"),
        P(EP, None, "tp"),
        P(EP, None, None, "tp"),
        P(None, "tp"),
        P(None, None, "tp"),
        P(EP, "tp", None),
        P("tp"),
        P("tp"),
        P("tp"),
        P("tp", EP),
        P(),
        P(None, EP_TP),
        P(None, EP_TP),
        P(EP_TP, None),
        P(),
        P(),
        P(),
        P(),
        P(EP, None, "tp"),
        P(EP, None, "tp"),
        P(EP, "tp", None),
    )
    out_specs = (P(EP_TP, None), P(EP, "tp", None))
    return jax.shard_map(
        shards, mesh=finer, in_specs=in_specs, out_specs=out_specs, check_vma=False
    )
```

profile of v0, /device:TPU:8, one launch (start us, length us, event | category | flops | bytes accessed | tf_op | source)
XLA Modules:
  0.0 377.9 jit_solution(146625243671493132)
XLA Ops:
  7.2 12.7 %all_gather.12 = bf16[1024,64]{0,1:T(8,128)(2,1)S(1)} all-gather(bf16[1024,16]{0,1:T(8,128)(2,1)} %param.38), channel_id=1, replica_groups=mesh['ep_0'=8,'ep_1'=4,'ep_2'=4,'tp'=2] {'ep_2'}, dimensions={1}, use_global_device_ids=true | all-gather | bytes 163840 | tf_op jit(solution)/shard_map/all_gather | solution.py:20
  19.9 13.7 %all_gather.13 = bf16[1024,256]{0,1:T(8,128)(2,1)} all-gather(bf16[1024,64]{0,1:T(8,128)(2,1)S(1)} %all_gather.12), channel_id=1, replica_groups=mesh['ep_0'=8,'ep_1'=4,'ep_2'=4,'tp'=2] {'ep_1'}, dimensions={1}, use_global_device_ids=true | all-gather | bytes 655360 | tf_op jit(solution)/shard_map/all_gather | solution.py:20
  37.9 7.9 %reshape.179 = f32[16,16,64,64]{3,2,1,0:T(8,128)} reshape(f32[16,16,4096]{2,1,0:T(8,128)} %param.34) | data formatting | bytes 8388608 | tf_op jit(solution)/shard_map/reshape | solution.py:81
  46.1 8.6 %broadcast_multiply_fusion = (f32[16,16,64,64]{3,2,1,0:T(8,128)}, f32[16,16,64]{2,1,0:T(8,128)S(1)}) fusion(f32[16,16,64]{2,1,0:T(8,128)S(1)} %bitcast.42, f32[16,16,64]{2,1,0:T(8,128)S(1)} %multiply_multiply_fusion, f32[16,16,64]{2,1,0:T(8,128)S(1)} %bitcast.43, f32[16,16,64,64]{3,2,1,0:T(8,128)} %reshape.179, f32[16,16]{1,0:T(8,128)S(1)} %get-tuple-element.11), kind=kLoop, calls=%fused_computation.4 | loop fusion | flops 5226496 | bytes 8651776 | tf_op jit(solution)/shard_map/mul | solution.py:82
  55.0 35.4 %all-gather.3.cloned.1.call-done = bf16[1024,2048]{0,1:T(8,128)(2,1)} async-done(((bf16[1024,256]{0,1:T(8,128)(2,1)}), bf16[1024,2048]{0,1:T(8,128)(2,1)}) %all-gather.3.cloned.1.call-update) | async-done | bytes 4194320 | tf_op jit(solution)/shard_map/all_gather | solution.py:20
  90.5 3.4 convolution_convert_fusion.2
  93.9 3.8 %all_to_all.20 = bf16[2,16,2048]{2,1,0:T(8,128)(2,1)S(1)} all-to-all(bf16[2,16,2048]{2,1,0:T(8,128)(2,1)S(1)} %broadcast_in_dim.21), channel_id=1, replica_groups=mesh['ep_0'=8,'ep_1'=4,'ep_2'=4,'tp'=2] {'tp'}, dimensions={0} | all-to-all | bytes 262144 | tf_op jit(solution)/shard_map/all_to_all | solution.py:26
  102.2 119.3 %all-gather.5.cloned.1.call-done = bf16[2048,2048]{1,0:T(8,128)(2,1)} async-done(((bf16[16,2048]{1,0:T(8,128)(2,1)}), bf16[2048,2048]{1,0:T(8,128)(2,1)}) %all-gather.5.cloned.1.call-update) | async-done | bytes 8388624 | tf_op jit(solution)/shard_map/all_gather | solution.py:144
  221.5 5.6 %fusion.38 = f32[1,2048]{1,0:T(1,128)S(1)} fusion(bf16[2048,2048]{1,0:T(8,128)(2,1)} %all-gather.5.cloned.1.call-done, bf16[2048,1]{0,1:T(2,128)(2,1)S(1)} %reshape.193), kind=kOutput, calls=%fused_computation.84 | convolution fusion | flops 8388608 | bytes 8400896 | tf_op jit(solution)/shard_map/dot_general | solution.py:145
  227.2 6.8 %gather_fusion = bf16[256,2048]{1,0:T(8,128)(2,1)S(1)} fusion(bf16[2048,2048]{1,0:T(8,128)(2,1)} %all-gather.5.cloned.1.call-done, s32[1024]{0:T(1024)S(1)} %pad_clamp_fusion), kind=kCustom, calls=%fused_computation | custom fusion | bytes 2098176 | tf_op jit(solution)/shard_map/jit(_take)/gather | solution.py:173
  234.0 2.4 fusion.9
  238.9 5.7 %fusion.39 = f32[2048,16]{0,1:T(8,128)S(1)} fusion(bf16[2048,2048]{1,0:T(8,128)(2,1)} %all-gather.5.cloned.1.call-done, bf16[2048,16]{0,1:T(8,128)(2,1)S(1)} %copy-done.3), kind=kOutput, calls=%fused_computation.85 | convolution fusion | flops 134217728 | bytes 8585216 | tf_op jit(solution)/shard_map/dot_general | solution.py:146
  244.5 5.7 %fusion = bf16[2048,16]{0,1:T(8,128)(2,1)S(1)} fusion(bf16[2048,2048]{1,0:T(8,128)(2,1)} %all-gather.5.cloned.1.call-done, bf16[2048,16]{0,1:T(8,128)(2,1)S(1)} %copy-done.7, f32[2048,16]{0,1:T(8,128)S(1)} %fusion.39, f32[2048]{0:T(1024)S(1)} %add_divide_fusion), kind=kOutput, calls=%fused_computation.8 | convolution fusion | flops 134447104 | bytes 8658944 | tf_op jit(solution)/shard_map/dot_general | solution.py:147
  253.4 4.7 %convolution_convert_fusion = bf16[2048,2048]{1,0:T(8,128)(2,1)S(1)} fusion(bf16[2048,272]{1,0:T(8,128)(2,1)S(1)} %bitcast.41, bf16[256,2048]{1,0:T(8,128)(2,1)S(1)} %bitcast.50, bf16[16,2048]{1,0:T(8,128)(2,1)S(1)} %copy-done.15), kind=kOutput, calls=%fused_computation.2 | convolution fusion | flops 2288123904 | bytes 10616832 | tf_op jit(solution)/shard_map/dot_general | solution.py:192
  258.1 11.7 %all_to_all.21 = bf16[2,1024,2048]{2,1,0:T(8,128)(2,1)} all-to-all(bf16[2,1024,2048]{2,1,0:T(8,128)(2,1)S(1)} %bitcast.39), channel_id=1, replica_groups=mesh['ep_0'=8,'ep_1'=4,'ep_2'=4,'tp'=2] {'tp'}, dimensions={0} | all-to-all | bytes 16777216 | tf_op jit(solution)/shard_map/all_to_all | solution.py:41
  269.9 8.8 %reduce_sum.139 = bf16[1024,2048]{1,0:T(8,128)(2,1)} reduce(bf16[2,1024,2048]{2,1,0:T(8,128)(2,1)} %all_to_all.21, bf16[]{:T(256)} %constant.95.clone.1), dimensions={0}, to_apply=%region_11.12 | reduce | flops 2097152 | bytes 12582914 | tf_op jit(solution)/shard_map/reduce_sum | solution.py:42
  278.6 4.7 %copy.59 = bf16[16,8,8,2048]{3,2,1,0:T(8,128)(2,1)} copy(bf16[16,8,8,2048]{3,2,0,1:T(8,128)(2,1)} %bitcast.38) | data formatting | bytes 8388608 | tf_op jit(solution)/shard_map/transpose | solution.py:36
  283.4 5.7 %all-to-all-start.2 = ((bf16[16,8,8,2048]{3,2,1,0:T(8,128)(2,1)}), bf16[16,8,8,2048]{3,2,1,0:T(8,128)(2,1)}, u32[]{:S(2)}, u32[]{:S(2)}) async-start(bf16[16,8,8,2048]{3,2,1,0:T(8,128)(2,1)} %copy.59), calls=%async_computation.2 | async-start | bytes 8388608 | tf_op jit(solution)/shard_map/all_to_all | solution.py:41
  289.1 7.9 %mul.296 = f32[16,16,4096]{2,1,0:T(8,128)} reshape(f32[16,16,64,64]{3,2,1,0:T(8,128)} %get-tuple-element.6) | data formatting | bytes 8388608 | tf_op jit(solution)/shard_map/mul | solution.py:82
  297.0 54.5 %all-to-all-done.2 = bf16[16,8,8,2048]{3,2,1,0:T(8,128)(2,1)} async-done(((bf16[16,8,8,2048]{3,2,1,0:T(8,128)(2,1)}), bf16[16,8,8,2048]{3,2,1,0:T(8,128)(2,1)}, u32[]{:S(2)}, u32[]{:S(2)}) %all-to-all-start.2) | async-done | bytes 4194336 | tf_op jit(solution)/shard_map/all_to_all | solution.py:41
  351.4 3.7 reduce_sum.140
  355.2 4.1 %all-to-all-start.3 = ((bf16[8,8,2048]{2,1,0:T(8,128)(2,1)}), bf16[8,8,2048]{2,1,0:T(8,128)(2,1)S(1)}, u32[]{:S(2)}, u32[]{:S(2)}) async-start(bf16[8,8,2048]{2,1,0:T(8,128)(2,1)} %reduce_sum.140), calls=%async_computation.3 | async-start | bytes 524288 | tf_op jit(solution)/shard_map/all_to_all | solution.py:49
  359.3 6.6 %multiply_add_fusion = f32[16,16,4096]{2,1,0:T(8,128)} fusion(f32[16,16,4096]{2,1,0:T(8,128)} %mul.296, f32[16,16,4096]{2,1,0:T(8,128)} %param.34, f32[16,16]{1,0:T(8,128)S(1)} %get-tuple-element.11), kind=kLoop, calls=%fused_computation.3 | loop fusion | flops 2097152 | bytes 12583936 | tf_op jit(solution)/shard_map/add | solution.py:83
  365.9 4.4 %all-to-all-done.3 = bf16[8,8,2048]{2,1,0:T(8,128)(2,1)S(1)} async-done(((bf16[8,8,2048]{2,1,0:T(8,128)(2,1)}), bf16[8,8,2048]{2,1,0:T(8,128)(2,1)S(1)}, u32[]{:S(2)}, u32[]{:S(2)}) %all-to-all-start.3) | async-done | bytes 262176 | tf_op jit(solution)/shard_map/all_to_all | solution.py:49
  (97 shorter events, 15.3 us)
Async XLA Ops:
  7.2 229.3 %copy-start = (bf16[1,2048,256]{2,1,0:T(8,128)(2,1)S(1)}, bf16[1,2048,256]{2,1,0:T(8,128)(2,1)}, u32[]{:S(2)}) copy-start(bf16[1,2048,256]{2,1,0:T(8,128)(2,1)} %param.48) | copy-start | bytes 3145732
  7.2 83.3 %all-gather.3.cloned.1.call-start = ((), (), s32[]{:S(2)}) async-start(), calls=%async_computation.4 | async-start | bytes 4718592 | tf_op jit(solution)/shard_map/all_gather | solution.py:20
  33.7 187.8 %all-gather.5.cloned.1.call-start = ((), (), s32[]{:S(2)}) async-start(), calls=%async_computation.5 | async-start | bytes 8454144 | tf_op jit(solution)/shard_map/all_gather | solution.py:144
  37.9 7.9 %copy-start.12 = (bf16[16,16]{1,0:T(8,128)(2,1)S(1)}, bf16[16,16]{1,0:T(8,128)(2,1)}, u32[]{:S(2)}) copy-start(bf16[16,16]{1,0:T(8,128)(2,1)} %param.29) | copy-start | bytes 1540
  37.9 7.9 %copy-start.13 = (f32[16]{0:T(128)S(1)}, f32[16]{0:T(128)}, u32[]{:S(2)}) copy-start(f32[16]{0:T(128)} %param.35) | copy-start | bytes 196
  46.0 8.7 %copy-start.2 = (bf16[16,1024]{1,0:T(8,128)(2,1)S(1)}, bf16[16,1024]{1,0:T(8,128)(2,1)}, u32[]{:S(2)}) copy-start(bf16[16,1024]{1,0:T(8,128)(2,1)} %param.27) | copy-start | bytes 98308
  46.0 44.4 %copy-start.10 = (f32[1024]{0:T(1024)S(1)}, f32[1024]{0:T(1024)}, u32[]{:S(2)}) copy-start(f32[1024]{0:T(1024)} %param.37) | copy-start | bytes 12292
  54.6 43.1 %copy-start.4 = (bf16[16,2048]{1,0:T(8,128)(2,1)S(1)}, bf16[16,2048]{1,0:T(8,128)(2,1)}, u32[]{:S(2)}) copy-start(bf16[16,2048]{1,0:T(8,128)(2,1)} %param.25) | copy-start | bytes 196612
  54.6 43.3 %copy-start.9 = (f32[2048]{0:T(1024)S(1)}, f32[2048]{0:T(1024)}, u32[]{:S(2)}) copy-start(f32[2048]{0:T(1024)} %param.39) | copy-start | bytes 24580
  54.6 44.1 %copy-start.5 = (s32[2048,6]{0,1:T(8,128)S(1)}, s32[2048,6]{0,1:T(8,128)}, u32[]{:S(2)}) copy-start(s32[2048,6]{0,1:T(8,128)} %param.45) | copy-start | bytes 147460
  90.4 9.9 %copy-start.11 = (bf16[2048]{0:T(1024)(128)(2,1)S(1)}, bf16[2048]{0:T(1024)(128)(2,1)}, u32[]{:S(2)}) copy-start(bf16[2048]{0:T(1024)(128)(2,1)} %param.43) | copy-start | bytes 12292
  90.4 10.3 %copy-start.8 = (f32[2048,4]{0,1:T(4,128)S(1)}, f32[2048,4]{0,1:T(4,128)}, u32[]{:S(2)}) copy-start(f32[2048,4]{0,1:T(4,128)} %param.44) | copy-start | bytes 98308
  90.4 10.4 %copy-start.6 = (f32[2048,6]{0,1:T(8,128)S(1)}, f32[2048,6]{0,1:T(8,128)}, u32[]{:S(2)}) copy-start(f32[2048,6]{0,1:T(8,128)} %param.46) | copy-start | bytes 147460
  234.0 4.8 %copy-start.3 = (bf16[2048,16]{0,1:T(8,128)(2,1)S(1)}, bf16[2048,16]{0,1:T(8,128)(2,1)}, u32[]{:S(2)}) copy-start(bf16[2048,16]{0,1:T(8,128)(2,1)} %param.40) | copy-start | bytes 196612
  238.8 5.7 %copy-start.7 = (bf16[2048,16]{0,1:T(8,128)(2,1)S(1)}, bf16[2048,16]{0,1:T(8,128)(2,1)}, u32[]{:S(2)}) copy-start(bf16[2048,16]{0,1:T(8,128)(2,1)} %param.41) | copy-start | bytes 196612
  250.2 3.1 copy-start.15
  251.3 2.1 copy-start.14
  283.4 68.1 %all-to-all-start.2 = ((bf16[16,8,8,2048]{3,2,1,0:T(8,128)(2,1)}), bf16[16,8,8,2048]{3,2,1,0:T(8,128)(2,1)}, u32[]{:S(2)}, u32[]{:S(2)}) async-start(bf16[16,8,8,2048]{3,2,1,0:T(8,128)(2,1)} %copy.59), calls=%async_computation.2 | async-start | bytes 8388608 | tf_op jit(solution)/shard_map/all_to_all | solution.py:41
  355.2 15.2 %all-to-all-start.3 = ((bf16[8,8,2048]{2,1,0:T(8,128)(2,1)}), bf16[8,8,2048]{2,1,0:T(8,128)(2,1)S(1)}, u32[]{:S(2)}, u32[]{:S(2)}) async-start(bf16[8,8,2048]{2,1,0:T(8,128)(2,1)} %reduce_sum.140), calls=%async_computation.3 | async-start | bytes 524288 | tf_op jit(solution)/shard_map/all_to_all | solution.py:49
  359.3 11.8 %copy-start.1 = (bf16[1,2048,256]{2,1,0:T(8,128)(2,1)S(1)}, bf16[1,2048,256]{2,1,0:T(8,128)(2,1)}, u32[]{:S(2)}) copy-start(bf16[1,2048,256]{2,1,0:T(8,128)(2,1)} %param.48) | copy-start | bytes 3145732
Sparse Core Ops, SparseCore 0:
  33.8 56.5 all-gather.2
  98.8 122.6 all-gather.4
where the time goes:
time: 379 us; the launch traced here: 378 us
  waiting for transfers between devices  214 us (56%)
  blocking collectives  42 us (11%)
  other arithmetic  34.4 us (9%)
  local copies, waits for them, and re-layouts  33.5 us (9%)
  matrix products  29.9 us (8%)
  between operations  14.5 us (4%)
  starting transfers between devices  9.92 us (3%)
    all_gather x1, waiting for transfers between devices, shards(): gathered = lax.all_gather(normed, EP, axis=0, tiled=True)  119 us
    all_to_all x1, waiting for transfers between devices, sum_at_owner(): lax.all_to_all(split_up(shard, dim, devices), axis, 0, 0, tiled=True)  54.5 us
    all_gather x1, waiting for transfers between devices, gathered_by_axis(): nearer = lax.all_gather(shard, axes[-1], axis=dim, tiled=True)  35.4 us
    all_gather x2, blocking collectives, gathered_by_axis(): nearer = lax.all_gather(shard, axes[-1], axis=dim, tiled=True)  26.4 us
    reduce_sum x2, other arithmetic, sum_at_owner(): return jnp.sum(pieces.astype(jnp.float32), axis=0)  12.5 us
    all_to_all x1, blocking collectives, sum_at_owner(): lax.all_to_all(split_up(shard, dim, devices), axis, 0, 0, tiled=True)  11.7 us
    mul x1, other arithmetic, state_update(): (step_size[:, :, None] * x_heads)[:, :, :, None]  8.56 us
    mul x1, local copies, waits for them, and re-layouts, state_update(): (step_size[:, :, None] * x_heads)[:, :, :, None]  7.88 us
  transfers between devices with their start and end apart: 4, of which 4 were waited for; matrix products, arithmetic and copies ran while one was open for 10% of the time, Pallas kernels for 0%

commit v1 on v0

--- a/solution.py
+++ b/solution.py
@@ -12,6 +12,13 @@
 EP = ("ep_0", "ep_1", "ep_2")
 EP_TP = ("ep_0", "ep_1", "ep_2", "tp")
 EPSILON = 1e-06
+
+
+def all_by_exchange(x, mesh_axis, along):
+    size = lax.axis_size(mesh_axis)
+    blocks = jnp.stack([x for _ in range(size)])
+    blocks = lax.all_to_all(blocks, mesh_axis, split_axis=0, concat_axis=0)
+    return jnp.concatenate(blocks, axis=along)
 
 
 def gathered_by_axis(shard, axes, dim):
@@ -141,7 +148,7 @@
         * lax.rsqrt(jnp.mean(widened * widened, axis=-1, keepdims=True) + EPSILON)
         * ffn_gain
     ).astype(jnp.bfloat16)
-    gathered = lax.all_gather(normed, EP, axis=0, tiled=True)
+    gathered = all_by_exchange(normed, EP, 0)
     score = jnp.dot(gathered, branch_gate, preferred_element_type=jnp.float32)
     dense_pre = jnp.dot(gathered, dense_gate, preferred_element_type=jnp.float32)
     dense_lin = jnp.dot(gathered, dense_up, preferred_element_type=jnp.float32)

time: 379 us -> 458 us (1.21)
  waiting for transfers between devices: 214 us -> 279 us
  starting transfers between devices: 9.92 us -> 20.6 us
    all_to_all x0 -> x1, waiting for transfers between devices: none -> 184 us  [all_by_exchange(): blocks = lax.all_to_all(blocks, mesh_axis, split_axis=0, concat_axis=0)]
    all_gather x1 -> x0, waiting for transfers between devices: 119 us -> none  [shards(): gathered = lax.all_gather(normed, EP, axis=0, tiled=True)]
    all_to_all x0 -> x1, starting transfers between devices: none -> 11.7 us  [all_by_exchange(): blocks = lax.all_to_all(blocks, mesh_axis, split_axis=0, concat_axis=0)]
  transfers between devices with their start and end apart: 4 -> 4, of which waited for: 4 -> 4; matrix products, arithmetic and copies ran while one was open for 10% -> 9% of each run, Pallas kernels for 0% -> 0%
where the time goes in v1:
time: 458 us; the launch traced here: 457 us
  waiting for transfers between devices  279 us (61%)
  blocking collectives  42 us (9%)
  local copies, waits for them, and re-layouts  37.7 us (8%)
  other arithmetic  33.8 us (7%)
  matrix products  28.8 us (6%)
  starting transfers between devices  20.6 us (4%)
  between operations  14.5 us (3%)
    all_to_all x1, waiting for transfers between devices, all_by_exchange(): blocks = lax.all_to_all(blocks, mesh_axis, split_axis=0, concat_axis=0)  184 us
    all_to_all x1, waiting for transfers between devices, sum_at_owner(): lax.all_to_all(split_up(shard, dim, devices), axis, 0, 0, tiled=True)  55.2 us
    all_gather x1, waiting for transfers between devices, gathered_by_axis(): nearer = lax.all_gather(shard, axes[-1], axis=dim, tiled=True)  35.5 us
    all_gather x2, blocking collectives, gathered_by_axis(): nearer = lax.all_gather(shard, axes[-1], axis=dim, tiled=True)  26.4 us
    reduce_sum x2, other arithmetic, sum_at_owner(): return jnp.sum(pieces.astype(jnp.float32), axis=0)  12.5 us
    all_to_all x1, blocking collectives, sum_at_owner(): lax.all_to_all(split_up(shard, dim, devices), axis, 0, 0, tiled=True)  11.7 us
    all_to_all x1, starting transfers between devices, all_by_exchange(): blocks = lax.all_to_all(blocks, mesh_axis, split_axis=0, concat_axis=0)  11.7 us
  transfers between devices with their start and end apart: 4, of which 4 were waited for; matrix products, arithmetic and copies ran while one was open for 9% of the time, Pallas kernels for 0%

profile of v1, /device:TPU:8, one launch (start us, length us, event | category | flops | bytes accessed | tf_op | source)
XLA Modules:
  0.0 456.6 jit_solution(13211266088590396823)
XLA Ops:
  7.2 12.7 %all_gather.9 = bf16[1024,64]{0,1:T(8,128)(2,1)S(1)} all-gather(bf16[1024,16]{0,1:T(8,128)(2,1)} %param.38), channel_id=1, replica_groups=mesh['ep_0'=8,'ep_1'=4,'ep_2'=4,'tp'=2] {'ep_2'}, dimensions={1}, use_global_device_ids=true | all-gather | bytes 163840 | tf_op jit(solution)/shard_map/all_gather | solution.py:27
  19.9 13.7 %all_gather.10 = bf16[1024,256]{0,1:T(8,128)(2,1)} all-gather(bf16[1024,64]{0,1:T(8,128)(2,1)S(1)} %all_gather.9), channel_id=1, replica_groups=mesh['ep_0'=8,'ep_1'=4,'ep_2'=4,'tp'=2] {'ep_1'}, dimensions={1}, use_global_device_ids=true | all-gather | bytes 655360 | tf_op jit(solution)/shard_map/all_gather | solution.py:27
  37.8 7.9 %reshape.184 = f32[16,16,64,64]{3,2,1,0:T(8,128)} reshape(f32[16,16,4096]{2,1,0:T(8,128)} %param.34) | data formatting | bytes 8388608 | tf_op jit(solution)/shard_map/reshape | solution.py:88
  46.0 8.6 %broadcast_multiply_fusion = (f32[16,16,64,64]{3,2,1,0:T(8,128)}, f32[16,16,64]{2,1,0:T(8,128)S(1)}) fusion(f32[16,16,64]{2,1,0:T(8,128)S(1)} %bitcast.43, f32[16,16,64]{2,1,0:T(8,128)S(1)} %multiply_multiply_fusion, f32[16,16,64]{2,1,0:T(8,128)S(1)} %bitcast.44, f32[16,16,64,64]{3,2,1,0:T(8,128)} %reshape.184, f32[16,16]{1,0:T(8,128)S(1)} %get-tuple-element.11), kind=kLoop, calls=%fused_computation.4 | loop fusion | flops 5226496 | bytes 8651776 | tf_op jit(solution)/shard_map/mul | solution.py:89
  55.0 35.5 %all-gather.2.cloned.1.call-done = bf16[1024,2048]{0,1:T(8,128)(2,1)} async-done(((bf16[1024,256]{0,1:T(8,128)(2,1)}), bf16[1024,2048]{0,1:T(8,128)(2,1)}) %all-gather.2.cloned.1.call-update) | async-done | bytes 4194320 | tf_op jit(solution)/shard_map/all_gather | solution.py:27
  93.8 3.8 all_to_all.25
  98.0 4.3 stack.2
  102.2 11.7 %all-to-all-start.1 = ((bf16[128,16,2048]{2,1,0:T(8,128)(2,1)}), bf16[128,16,2048]{2,1,0:T(8,128)(2,1)}, u32[]{:S(2)}, u32[]{:S(2)}) async-start(bf16[128,16,2048]{2,1,0:T(8,128)(2,1)} %stack.2), calls=%async_computation.1 | async-start | bytes 16777216 | tf_op jit(solution)/shard_map/all_to_all | solution.py:20
  117.5 183.7 %all-to-all-done.1 = bf16[128,16,2048]{2,1,0:T(8,128)(2,1)} async-done(((bf16[128,16,2048]{2,1,0:T(8,128)(2,1)}), bf16[128,16,2048]{2,1,0:T(8,128)(2,1)}, u32[]{:S(2)}, u32[]{:S(2)}) %all-to-all-start.1) | async-done | bytes 8388640 | tf_op jit(solution)/shard_map/all_to_all | solution.py:20
  301.2 5.7 %fusion.38 = f32[1,2048]{1,0:T(1,128)S(1)} fusion(bf16[2048,2048]{1,0:T(8,128)(2,1)} %bitcast.6, bf16[2048,1]{0,1:T(2,128)(2,1)S(1)} %reshape.199), kind=kOutput, calls=%fused_computation.84 | convolution fusion | flops 8388608 | bytes 8400896 | tf_op jit(solution)/shard_map/dot_general | solution.py:152
  306.9 5.6 %fusion.39 = f32[2048,16]{0,1:T(8,128)S(1)} fusion(bf16[2048,2048]{1,0:T(8,128)(2,1)} %bitcast.6, bf16[2048,16]{0,1:T(8,128)(2,1)S(1)} %copy-done.3), kind=kOutput, calls=%fused_computation.85 | convolution fusion | flops 134217728 | bytes 8585216 | tf_op jit(solution)/shard_map/dot_general | solution.py:153
  312.5 6.9 %gather_fusion = bf16[256,2048]{1,0:T(8,128)(2,1)S(1)} fusion(bf16[2048,2048]{1,0:T(8,128)(2,1)} %bitcast.6, s32[1024]{0:T(1024)S(1)} %pad_clamp_fusion), kind=kCustom, calls=%fused_computation | custom fusion | bytes 2098176 | tf_op jit(solution)/shard_map/jit(_take)/gather | solution.py:180
  319.4 5.7 %fusion = bf16[2048,16]{0,1:T(8,128)(2,1)S(1)} fusion(bf16[2048,2048]{1,0:T(8,128)(2,1)} %bitcast.6, bf16[2048,16]{0,1:T(8,128)(2,1)S(1)} %copy-done.7, f32[2048,16]{0,1:T(8,128)S(1)} %fusion.39, f32[2048]{0:T(1024)S(1)} %add_divide_fusion), kind=kOutput, calls=%fused_computation.8 | convolution fusion | flops 134447104 | bytes 8658944 | tf_op jit(solution)/shard_map/dot_general | solution.py:154
  331.9 4.7 %convolution_convert_fusion = bf16[2048,2048]{1,0:T(8,128)(2,1)S(1)} fusion(bf16[2048,272]{1,0:T(8,128)(2,1)S(1)} %bitcast.42, bf16[256,2048]{1,0:T(8,128)(2,1)S(1)} %bitcast.51, bf16[16,2048]{1,0:T(8,128)(2,1)S(1)} %copy-done.16), kind=kOutput, calls=%fused_computation.2 | convolution fusion | flops 2288123904 | bytes 10616832 | tf_op jit(solution)/shard_map/dot_general | solution.py:199
  336.6 11.7 %all_to_all.26 = bf16[2,1024,2048]{2,1,0:T(8,128)(2,1)} all-to-all(bf16[2,1024,2048]{2,1,0:T(8,128)(2,1)S(1)} %bitcast.40), channel_id=1, replica_groups=mesh['ep_0'=8,'ep_1'=4,'ep_2'=4,'tp'=2] {'tp'}, dimensions={0} | all-to-all | bytes 16777216 | tf_op jit(solution)/shard_map/all_to_all | solution.py:48
  348.3 8.8 %reduce_sum.139 = bf16[1024,2048]{1,0:T(8,128)(2,1)} reduce(bf16[2,1024,2048]{2,1,0:T(8,128)(2,1)} %all_to_all.26, bf16[]{:T(256)} %constant.95.clone.1), dimensions={0}, to_apply=%region_11.12 | reduce | flops 2097152 | bytes 12582914 | tf_op jit(solution)/shard_map/reduce_sum | solution.py:49
  357.1 4.7 %copy.59 = bf16[16,8,8,2048]{3,2,1,0:T(8,128)(2,1)} copy(bf16[16,8,8,2048]{3,2,0,1:T(8,128)(2,1)} %bitcast.39) | data formatting | bytes 8388608 | tf_op jit(solution)/shard_map/transpose | solution.py:43
  361.9 5.5 %all-to-all-start.3 = ((bf16[16,8,8,2048]{3,2,1,0:T(8,128)(2,1)}), bf16[16,8,8,2048]{3,2,1,0:T(8,128)(2,1)}, u32[]{:S(2)}, u32[]{:S(2)}) async-start(bf16[16,8,8,2048]{3,2,1,0:T(8,128)(2,1)} %copy.59), calls=%async_computation.3 | async-start | bytes 8388608 | tf_op jit(solution)/shard_map/all_to_all | solution.py:48
  367.4 7.9 %mul.296 = f32[16,16,4096]{2,1,0:T(8,128)} reshape(f32[16,16,64,64]{3,2,1,0:T(8,128)} %get-tuple-element.6) | data formatting | bytes 8388608 | tf_op jit(solution)/shard_map/mul | solution.py:89
  375.2 55.2 %all-to-all-done.3 = bf16[16,8,8,2048]{3,2,1,0:T(8,128)(2,1)} async-done(((bf16[16,8,8,2048]{3,2,1,0:T(8,128)(2,1)}), bf16[16,8,8,2048]{3,2,1,0:T(8,128)(2,1)}, u32[]{:S(2)}, u32[]{:S(2)}) %all-to-all-start.3) | async-done | bytes 4194336 | tf_op jit(solution)/shard_map/all_to_all | solution.py:48
  430.5 3.7 reduce_sum.140
  434.2 3.4 all-to-all-start.4
  437.6 6.6 %multiply_add_fusion = f32[16,16,4096]{2,1,0:T(8,128)} fusion(f32[16,16,4096]{2,1,0:T(8,128)} %mul.296, f32[16,16,4096]{2,1,0:T(8,128)} %param.34, f32[16,16]{1,0:T(8,128)S(1)} %get-tuple-element.11), kind=kLoop, calls=%fused_computation.3 | loop fusion | flops 2097152 | bytes 12583936 | tf_op jit(solution)/shard_map/add | solution.py:90
  444.3 4.9 %all-to-all-done.4 = bf16[8,8,2048]{2,1,0:T(8,128)(2,1)S(1)} async-done(((bf16[8,8,2048]{2,1,0:T(8,128)(2,1)}), bf16[8,8,2048]{2,1,0:T(8,128)(2,1)S(1)}, u32[]{:S(2)}, u32[]{:S(2)}) %all-to-all-start.4) | async-done | bytes 262176 | tf_op jit(solution)/shard_map/all_to_all | solution.py:56
  (99 shorter events, 19.1 us)
Async XLA Ops:
  7.2 319.2 %copy-start = (bf16[1,2048,256]{2,1,0:T(8,128)(2,1)S(1)}, bf16[1,2048,256]{2,1,0:T(8,128)(2,1)}, u32[]{:S(2)}) copy-start(bf16[1,2048,256]{2,1,0:T(8,128)(2,1)} %param.48) | copy-start | bytes 3145732
  7.2 83.3 %all-gather.2.cloned.1.call-start = ((), (), s32[]{:S(2)}) async-start(), calls=%async_computation.5 | async-start | bytes 4718592 | tf_op jit(solution)/shard_map/all_gather | solution.py:27
  37.8 7.9 %copy-start.12 = (bf16[16,16]{1,0:T(8,128)(2,1)S(1)}, bf16[16,16]{1,0:T(8,128)(2,1)}, u32[]{:S(2)}) copy-start(bf16[16,16]{1,0:T(8,128)(2,1)} %param.29) | copy-start | bytes 1540
  37.8 7.9 %copy-start.13 = (f32[16]{0:T(128)S(1)}, f32[16]{0:T(128)}, u32[]{:S(2)}) copy-start(f32[16]{0:T(128)} %param.35) | copy-start | bytes 196
  46.0 8.7 %copy-start.2 = (bf16[16,1024]{1,0:T(8,128)(2,1)S(1)}, bf16[16,1024]{1,0:T(8,128)(2,1)}, u32[]{:S(2)}) copy-start(bf16[16,1024]{1,0:T(8,128)(2,1)} %param.27) | copy-start | bytes 98308
  46.0 44.4 %copy-start.10 = (f32[1024]{0:T(1024)S(1)}, f32[1024]{0:T(1024)}, u32[]{:S(2)}) copy-start(f32[1024]{0:T(1024)} %param.37) | copy-start | bytes 12292
  54.6 43.1 %copy-start.4 = (bf16[16,2048]{1,0:T(8,128)(2,1)S(1)}, bf16[16,2048]{1,0:T(8,128)(2,1)}, u32[]{:S(2)}) copy-start(bf16[16,2048]{1,0:T(8,128)(2,1)} %param.25) | copy-start | bytes 196612
  54.6 43.3 %copy-start.9 = (f32[2048]{0:T(1024)S(1)}, f32[2048]{0:T(1024)}, u32[]{:S(2)}) copy-start(f32[2048]{0:T(1024)} %param.39) | copy-start | bytes 24580
  102.2 11.7 %copy-start.5 = (s32[2048,6]{0,1:T(8,128)S(1)}, s32[2048,6]{0,1:T(8,128)}, u32[]{:S(2)}) copy-start(s32[2048,6]{0,1:T(8,128)} %param.45) | copy-start | bytes 147460
  102.2 13.4 %copy-start.11 = (bf16[2048]{0:T(1024)(128)(2,1)S(1)}, bf16[2048]{0:T(1024)(128)(2,1)}, u32[]{:S(2)}) copy-start(bf16[2048]{0:T(1024)(128)(2,1)} %param.43) | copy-start | bytes 12292
  102.2 13.7 %copy-start.8 = (f32[2048,4]{0,1:T(4,128)S(1)}, f32[2048,4]{0,1:T(4,128)}, u32[]{:S(2)}) copy-start(f32[2048,4]{0,1:T(4,128)} %param.44) | copy-start | bytes 98308
  102.2 13.8 %copy-start.6 = (f32[2048,6]{0,1:T(8,128)S(1)}, f32[2048,6]{0,1:T(8,128)}, u32[]{:S(2)}) copy-start(f32[2048,6]{0,1:T(8,128)} %param.46) | copy-start | bytes 147460
  102.2 198.9 %all-to-all-start.1 = ((bf16[128,16,2048]{2,1,0:T(8,128)(2,1)}), bf16[128,16,2048]{2,1,0:T(8,128)(2,1)}, u32[]{:S(2)}, u32[]{:S(2)}) async-start(bf16[128,16,2048]{2,1,0:T(8,128)(2,1)} %stack.2), calls=%async_computation.1 | async-start | bytes 16777216 | tf_op jit(solution)/shard_map/all_to_all | solution.py:20
  301.2 5.7 %copy-start.3 = (bf16[2048,16]{0,1:T(8,128)(2,1)S(1)}, bf16[2048,16]{0,1:T(8,128)(2,1)}, u32[]{:S(2)}) copy-start(bf16[2048,16]{0,1:T(8,128)(2,1)} %param.40) | copy-start | bytes 196612
  312.5 6.9 %copy-start.7 = (bf16[2048,16]{0,1:T(8,128)(2,1)S(1)}, bf16[2048,16]{0,1:T(8,128)(2,1)}, u32[]{:S(2)}) copy-start(bf16[2048,16]{0,1:T(8,128)(2,1)} %param.41) | copy-start | bytes 196612
  319.4 5.8 %copy-start.14 = (bf16[1,2048,256]{2,1,0:T(8,128)(2,1)S(1)}, bf16[1,2048,256]{2,1,0:T(8,128)(2,1)}, u32[]{:S(2)}) copy-start(bf16[1,2048,256]{2,1,0:T(8,128)(2,1)} %param.47) | copy-start | bytes 3145732
  328.8 3.1 copy-start.15
  328.8 3.1 copy-start.16
  361.9 68.6 %all-to-all-start.3 = ((bf16[16,8,8,2048]{3,2,1,0:T(8,128)(2,1)}), bf16[16,8,8,2048]{3,2,1,0:T(8,128)(2,1)}, u32[]{:S(2)}, u32[]{:S(2)}) async-start(bf16[16,8,8,2048]{3,2,1,0:T(8,128)(2,1)} %copy.59), calls=%async_computation.3 | async-start | bytes 8388608 | tf_op jit(solution)/shard_map/all_to_all | solution.py:48
  434.2 14.9 %all-to-all-start.4 = ((bf16[8,8,2048]{2,1,0:T(8,128)(2,1)}), bf16[8,8,2048]{2,1,0:T(8,128)(2,1)S(1)}, u32[]{:S(2)}, u32[]{:S(2)}) async-start(bf16[8,8,2048]{2,1,0:T(8,128)(2,1)} %reduce_sum.140), calls=%async_computation.4 | async-start | bytes 524288 | tf_op jit(solution)/shard_map/all_to_all | solution.py:56
  437.6 12.2 %copy-start.1 = (bf16[1,2048,256]{2,1,0:T(8,128)(2,1)S(1)}, bf16[1,2048,256]{2,1,0:T(8,128)(2,1)}, u32[]{:S(2)}) copy-start(bf16[1,2048,256]{2,1,0:T(8,128)(2,1)} %param.48) | copy-start | bytes 3145732
Sparse Core Ops, SparseCore 0:
  33.8 56.5 all-gather.1
